TPU v7x, 32 devices: a whole 2x2x4 slice. The times are simulated.
32 devices in a mesh: tp: 4 (over y, x), dp: 8 (over z, core).
Axes of the slice: x: 2, y: 2, z: 4, core: 2. Of those that a mesh axis runs over, the one named last changes fastest.
Arguments:
- tokens: bfloat16 [128, 4096], P(None, 'dp'), may hold values from -15 to 15, as said below
- norm_gain: float32 [2, 4096], P(None, 'dp'), may hold values from 0.1 to 1.9
- w_query: bfloat16 [2, 4096, 2048], P(None, 'dp', 'tp'), may hold values from -0.09375 to 0.09375
- w_forget: bfloat16 [2, 4096, 2048], P(None, 'dp', 'tp'), may hold values from -0.09375 to 0.09375
- w_value: bfloat16 [2, 4096, 2048], P(None, 'dp', 'tp'), may hold values from -0.09375 to 0.09375
- w_gate: bfloat16 [2, 4096, 2048], P(None, 'dp', 'tp'), may hold values from -0.09375 to 0.09375
- floor_rate: float32 [2, 2048], P(None, 'tp'), may hold values from 0 to 0.9
- head_gain: float32 [2, 128], replicated, may hold values from 0.1 to 1.9
- w_output: bfloat16 [2, 2048, 4096], P(None, 'tp', 'dp'), may hold values from -0.3 to 0.3
- state: float32 [2, 128, 16, 128, 128], P(None, 'dp', 'tp'), may hold values from -4 to 4
Outputs:
- mixed: bfloat16 [128, 4096], P(None, 'dp')
- new_state: float32 [2, 128, 16, 128, 128], P(None, 'dp', 'tp')
Inputs may be any that keep to these rules, and one draw needn't show every extreme that they name: `tokens`: activations whose feature blocks have different scales.
All inputs are finite; a program needn't handle non-finite values.
Results may differ from a plain program's by a relative error of at most 0.035.
Values may be sent and summed in bfloat16 or wider, within the bound.
A program may use at most 64 MiB of HBM per device.

v0:
```python
import jax
import jax.numpy as jnp
from jax import lax
from jax.sharding import PartitionSpec as P

D = 4096
DK = 128


EPS = 1e-06


def mixer_layer(tokens, norm_gain, weights, floor_rate, head_gain, w_output, old_state):
    tok = tokens.astype(jnp.float32)
    squares = lax.psum_scatter(jnp.sum(tok * tok, axis=1), "dp", scatter_dimension=0, tiled=True)
    row_scale = lax.rsqrt(squares / D + EPS)
    normed = (tok * norm_gain).astype(jnp.bfloat16)
    own_rows = old_state.shape[0]
    outputs = []
    for partial_weight in weights:
        product = jnp.dot(normed, partial_weight, preferred_element_type=jnp.float32)
        outputs.append(lax.optimization_barrier(product.astype(jnp.bfloat16)).astype(jnp.float32))
    summed = lax.psum_scatter(
        jnp.concatenate(outputs, axis=1).astype(jnp.bfloat16), "dp", scatter_dimension=0, tiled=True
    ).astype(jnp.float32)
    stored = lax.optimization_barrier((row_scale[:, None] * summed).astype(jnp.bfloat16)).astype(
        jnp.float32
    )
    heads_dev = old_state.shape[1]
    widths = [weight.shape[1] for weight in weights]
    offsets = [0, widths[0], widths[0] + widths[1], widths[0] + widths[1] + widths[2]]
    pieces = [
        stored[:, offsets[n] : offsets[n] + widths[n]].reshape(own_rows, heads_dev, -1)
        for n in range(4)
    ]
    query = jax.nn.silu(pieces[0]) * DK ** (-0.5)
    forget_pre, value, gate_pre = (pieces[1], pieces[2], pieces[3])
    floor_heads = floor_rate.reshape(heads_dev, -1)
    forget = floor_heads + (1.0 - floor_heads) * jax.nn.sigmoid(forget_pre)
    key_in = (1.0 - floor_heads) * jax.nn.sigmoid(-forget_pre)
    updated = old_state * forget[..., None] + key_in[..., None] * value[:, :, None, :]
    read = jnp.einsum("bhk,bhkv->bhv", query, updated, precision=lax.Precision.HIGHEST)
    read = read * lax.rsqrt(jnp.mean(read * read, axis=-1, keepdims=True) + EPS) * head_gain
    gated = (read * jax.nn.silu(gate_pre)).reshape(own_rows, -1).astype(jnp.bfloat16)
    partial_update = jnp.dot(
        lax.all_gather(gated, "dp", axis=0, tiled=True),
        w_output,
        preferred_element_type=jnp.float32,
    )
    share = lax.psum_scatter(
        partial_update.astype(jnp.bfloat16), "tp", scatter_dimension=0, tiled=True
    ).astype(jnp.float32)
    share_rows = share.shape[0]
    own_tok = lax.dynamic_slice_in_dim(tok, lax.axis_index("tp") * share_rows, share_rows, 0)
    fresh = (own_tok + share).astype(jnp.bfloat16)
    result = lax.all_gather(fresh, "tp", axis=0, tiled=True)
    return (result, updated)


def per_device(
    tokens, norm_gain, w_query, w_forget, w_value, w_gate, floor_rate, head_gain, w_output, state
):
    current = tokens
    states = []
    for layer_index in range(2):
        weights = (
            w_query[layer_index],
            w_forget[layer_index],
            w_value[layer_index],
            w_gate[layer_index],
        )
        current, updated = mixer_layer(
            current,
            norm_gain[layer_index],
            weights,
            floor_rate[layer_index],
            head_gain[layer_index],
            w_output[layer_index],
            state[layer_index],
        )
        states.append(updated)
    return (current, jnp.stack(states, axis=0))


def solution(mesh):
    in_specs = (
        P(None, "dp"),
        P(None, "dp"),
        P(None, "dp", "tp"),
        P(None, "dp", "tp"),
        P(None, "dp", "tp"),
        P(None, "dp", "tp"),
        P(None, "tp"),
        P(),
        P(None, "tp", "dp"),
        P(None, "dp", "tp", None, None),
    )
    out_specs = (P(None, "dp"), P(None, "dp", "tp", None, None))
    return jax.shard_map(
        per_device, mesh=mesh, in_specs=in_specs, out_specs=out_specs, check_vma=False
    )
```

profile of v0, /device:TPU:0, one launch (start us, length us, event | category | flops | bytes accessed | tf_op | source)
XLA Modules:
  0.0 212.2 jit_solution(17944524527027223087)
XLA Ops:
  7.3 0.8 fusion.49
  8.0 1.3 convolution_convert_fusion.8
  9.4 1.3 convolution_convert_fusion.7
  10.7 1.3 convolution_convert_fusion.6
  12.1 1.3 convolution_convert_fusion.9
  13.4 0.8 pad_maximum_fusion.1
  14.4 0.6 dynamic-slice
  15.7 18.2 %all-reduce = f32[128]{0:T(128)S(1)} all-reduce(f32[128]{0:T(128)S(1)} %multiply_reduce_fusion.1), channel_id=2, replica_groups=mesh['tp'=4,'dp'=8] {'dp'}, use_global_device_ids=true, to_apply=%region_1.0.clone | all-reduce | flops 128 | bytes 1024
  34.0 14.5 %reduce-scatter.5.cloned.1.call-done = bf16[16,2048]{1,0:T(8,128)(2,1)} async-done(((bf16[128,2048]{1,0:T(8,128)(2,1)}), bf16[16,2048]{1,0:T(8,128)(2,1)}) %reduce-scatter.5.cloned.1.call-update) | async-done | bytes 65552 | tf_op jit(solution)/shard_map/reduce_scatter | solution.py:23
  48.6 0.9 multiply_convert_fusion.3
  49.7 6.9 %fusion.4 = f32[16,4,1,128]{3,2,1,0:T(1,128)S(1)} fusion(f32[16,4,128,1]{2,3,1,0:T(1,128)S(1)} %bitcast.104, f32[2,16,4,128,128]{4,3,2,1,0:T(8,128)} %param.19, f32[16,4,128]{2,1,0:T(4,128)S(1)} %mul.254, f32[16,4,128]{2,1,0:T(4,128)S(1)} %bitcast.85, f32[16,4,128]{2,1,0:T(4,128)S(1)} %bitcast.83), kind=kOutput, calls=%fused_computation.6 | convolution fusion | flops 15728640 | bytes 4358144 | tf_op jit(solution)/shard_map/bhk,bhkv->bhv/dot_general | solution.py:42
  56.8 14.0 %all_gather.12 = bf16[128,512]{1,0:T(8,128)(2,1)S(1)} all-gather(bf16[16,512]{1,0:T(8,128)(2,1)S(1)} %bitcast.99), channel_id=1, replica_groups=mesh['tp'=4,'dp'=8] {'dp'}, dimensions={0}, use_global_device_ids=true | all-gather | bytes 147456 | tf_op jit(solution)/shard_map/all_gather | solution.py:46
  70.8 1.9 convolution_convert_fusion.5
  72.8 22.4 %reduce-scatter.7.cloned.1.call-done = bf16[32,512]{1,0:T(8,128)(2,1)} async-done(((bf16[128,512]{1,0:T(8,128)(2,1)}), bf16[32,512]{1,0:T(8,128)(2,1)}) %reduce-scatter.7.cloned.1.call-update) | async-done | bytes 32784 | tf_op jit(solution)/shard_map/reduce_scatter | solution.py:50
  95.2 0.8 add_convert_fusion.1
  96.0 8.5 %all_gather.13 = bf16[128,512]{1,0:T(8,128)(2,1)S(1)} all-gather(bf16[32,512]{1,0:T(8,128)(2,1)S(1)} %add_convert_fusion.1), channel_id=1, replica_groups=mesh['tp'=4,'dp'=8] {'tp'}, dimensions={0}, use_global_device_ids=true | all-gather | bytes 163840 | tf_op jit(solution)/shard_map/all_gather | solution.py:56
  104.7 0.2 convolution_convert_fusion.2
  104.9 1.3 convolution_convert_fusion.1
  106.2 1.3 convolution_convert_fusion.4
  107.5 0.8 pad_maximum_fusion.2
  108.6 13.8 %all-reduce.1 = f32[128]{0:T(128)S(1)} all-reduce(f32[128]{0:T(128)S(1)} %multiply_reduce_fusion), channel_id=5, replica_groups=mesh['tp'=4,'dp'=8] {'dp'}, use_global_device_ids=true, to_apply=%region_6.7.clone | all-reduce | flops 128 | bytes 1024
  122.5 17.2 %reduce-scatter.9.cloned.1.call-done = bf16[16,2048]{1,0:T(8,128)(2,1)} async-done(((bf16[128,2048]{1,0:T(8,128)(2,1)}), bf16[16,2048]{1,0:T(8,128)(2,1)}) %reduce-scatter.9.cloned.1.call-update) | async-done | bytes 65552 | tf_op jit(solution)/shard_map/reduce_scatter | solution.py:23
  139.7 0.9 multiply_convert_fusion.2
  140.8 10.4 %multiply_add_fusion.1 = (f32[1,16,4,128,128]{4,3,2,1,0:T(8,128)}, f32[1,16,4,128,128]{4,3,2,1,0:T(8,128)}) fusion(f32[2,16,4,128,128]{4,3,2,1,0:T(8,128)} %param.19, f32[16,4,128]{2,1,0:T(4,128)S(1)} %mul.254, f32[16,4,128]{2,1,0:T(4,128)S(1)} %bitcast.86, f32[16,4,128]{2,1,0:T(4,128)S(1)} %bitcast.84, f32[16,4,128]{2,1,0:T(4,128)S(1)} %mul.279, ...), kind=kLoop, calls=%fused_computation.8 | loop fusion | flops 6291456 | bytes 16973824 | tf_op jit(solution)/shard_map/add | solution.py:41
  151.3 6.9 %fusion.1 = f32[16,4,1,128]{3,2,1,0:T(1,128)S(1)} fusion(f32[16,4,128,1]{2,3,1,0:T(1,128)S(1)} %bitcast.103, f32[2,16,4,128,128]{4,3,2,1,0:T(8,128)} %param.19, f32[16,4,128]{2,1,0:T(4,128)S(1)} %mul.279, f32[16,4,128]{2,1,0:T(4,128)S(1)} %bitcast.90, f32[16,4,128]{2,1,0:T(4,128)S(1)} %bitcast.88), kind=kOutput, calls=%fused_computation.3 | convolution fusion | flops 15728640 | bytes 4358144 | tf_op jit(solution)/shard_map/bhk,bhkv->bhv/dot_general | solution.py:42
  158.4 14.0 %all_gather.14 = bf16[128,512]{1,0:T(8,128)(2,1)S(1)} all-gather(bf16[16,512]{1,0:T(8,128)(2,1)S(1)} %bitcast.100), channel_id=1, replica_groups=mesh['tp'=4,'dp'=8] {'dp'}, dimensions={0}, use_global_device_ids=true | all-gather | bytes 147456 | tf_op jit(solution)/shard_map/all_gather | solution.py:46
  172.4 0.9 convolution_convert_fusion
  173.3 8.0 %pad_maximum_fusion = f32[2,16,4,128,128]{4,3,2,1,0:T(8,128)} fusion(f32[1,16,4,128,128]{4,3,2,1,0:T(8,128)} %get-tuple-element.3, f32[1,16,4,128,128]{4,3,2,1,0:T(8,128)} %get-tuple-element.2), kind=kLoop, calls=%fused_computation | loop fusion | flops 2097152 | bytes 16777216 | tf_op jit(solution)/shard_map/stack | solution.py:82
  181.2 14.5 %reduce-scatter.11.cloned.1.call-done = bf16[32,512]{1,0:T(8,128)(2,1)} async-done(((bf16[128,512]{1,0:T(8,128)(2,1)}), bf16[32,512]{1,0:T(8,128)(2,1)}) %reduce-scatter.11.cloned.1.call-update) | async-done | bytes 32784 | tf_op jit(solution)/shard_map/reduce_scatter | solution.py:50
  195.8 0.8 add_convert_fusion
  196.5 8.5 %all_gather.15 = bf16[128,512]{1,0:T(8,128)(2,1)S(1)} all-gather(bf16[32,512]{1,0:T(8,128)(2,1)S(1)} %add_convert_fusion), channel_id=1, replica_groups=mesh['tp'=4,'dp'=8] {'tp'}, dimensions={0}, use_global_device_ids=true | all-gather | bytes 163840 | tf_op jit(solution)/shard_map/all_gather | solution.py:56
  205.0 0.7 copy.23
  (65 shorter events, 1.7 us)
Async XLA Ops:
  7.2 7.2 %copy-start.6 = (u32[32]{0:T(128)S(1)}, u32[32]{0:T(128)}, u32[]{:S(2)}) copy-start(u32[32]{0:T(128)} %constant.36) | copy-start | bytes 388
  7.2 8.4 %copy-start = (bf16[128,512]{1,0:T(8,128)(2,1)S(1)}, bf16[128,512]{1,0:T(8,128)(2,1)}, u32[]{:S(2)}) copy-start(bf16[128,512]{1,0:T(8,128)(2,1)} %param.10) | copy-start | bytes 393220
  7.2 26.8 %copy-start.2 = (f32[2,128]{1,0:T(2,128)S(1)}, f32[2,128]{1,0:T(2,128)}, u32[]{:S(2)}) copy-start(f32[2,128]{1,0:T(2,128)} %param.17) | copy-start | bytes 3076
  7.2 26.8 %copy-start.1 = (f32[2,512]{1,0:T(2,128)S(1)}, f32[2,512]{1,0:T(2,128)}, u32[]{:S(2)}) copy-start(f32[2,512]{1,0:T(2,128)} %param.16) | copy-start | bytes 12292
  7.2 41.4 %reduce-scatter.5.cloned.1.call-start = ((), (), s32[]{:S(2)}) async-start(), calls=%async_computation.4 | async-start | bytes 589824 | tf_op jit(solution)/shard_map/reduce_scatter | solution.py:23
  14.3 90.2 %copy-start.3 = (bf16[2,512,512]{2,1,0:T(8,128)(2,1)S(1)}, bf16[2,512,512]{2,1,0:T(8,128)(2,1)}, u32[]{:S(2)}) copy-start(bf16[2,512,512]{2,1,0:T(8,128)(2,1)} %param.13) | copy-start | bytes 3145732
  14.3 80.9 %reduce-scatter.7.cloned.1.call-start = ((), (), s32[]{:S(2)}) async-start(), calls=%async_computation.5 | async-start | bytes 163840 | tf_op jit(solution)/shard_map/reduce_scatter | solution.py:50
  49.5 55.2 %copy-start.4 = (bf16[2,512,512]{2,1,0:T(8,128)(2,1)S(1)}, bf16[2,512,512]{2,1,0:T(8,128)(2,1)}, u32[]{:S(2)}) copy-start(bf16[2,512,512]{2,1,0:T(8,128)(2,1)} %param.14) | copy-start | bytes 3145732
  72.8 66.9 %reduce-scatter.9.cloned.1.call-start = ((), (), s32[]{:S(2)}) async-start(), calls=%async_computation.6 | async-start | bytes 589824 | tf_op jit(solution)/shard_map/reduce_scatter | solution.py:23
  108.4 87.4 %reduce-scatter.11.cloned.1.call-start = ((), (), s32[]{:S(2)}) async-start(), calls=%async_computation.7 | async-start | bytes 163840 | tf_op jit(solution)/shard_map/reduce_scatter | solution.py:50
  151.2 21.1 %copy-start.5 = (bf16[2,512,512]{2,1,0:T(8,128)(2,1)S(1)}, bf16[2,512,512]{2,1,0:T(8,128)(2,1)}, u32[]{:S(2)}) copy-start(bf16[2,512,512]{2,1,0:T(8,128)(2,1)} %param.18) | copy-start | bytes 3145732
Sparse Core Ops, SparseCore 0:
  14.4 34.0 reduce-scatter.4
  72.9 22.2 reduce-scatter.6
  108.5 31.1 reduce-scatter.8
  173.4 22.3 reduce-scatter.10
where the time goes:
time: 213 us; the launch traced here: 212 us
  blocking collectives  76.9 us (36%)
  waiting for transfers between devices  68.7 us (32%)
  matrix products  25 us (12%)
  other arithmetic  24.4 us (11%)
  between operations  14.8 us (7%)
  local copies, waits for them, and re-layouts  2.25 us (1%)
    reduce_scatter x2, waiting for transfers between devices, mixer_layer(): lax.psum_scatter(partial_update.astype(jnp.bfloat16), 'tp', scatter_dimen...  36.9 us
    unnamed x2, blocking collectives  32 us
    reduce_scatter x2, waiting for transfers between devices, mixer_layer(): lax.psum_scatter(jnp.concatenate(outputs, axis=1).astype(jnp.bfloat16), '...  31.7 us
    all_gather x2, blocking collectives, mixer_layer(): lax.all_gather(gated, 'dp', axis=0, tiled=True)  27.9 us
    all_gather x2, blocking collectives, mixer_layer(): result = lax.all_gather(fresh, 'tp', axis=0, tiled=True)  16.9 us
    dot_general x2, matrix products, mixer_layer(): jnp.einsum('bhk,bhkv->bhv', query, updated, precision=lax.Precision.HIGHEST)  13.8 us
    add x1, other arithmetic, mixer_layer(): old_state * forget[..., None] + key_in[..., None] * value[:, :, None, :]  10.4 us
    dot_general x8, matrix products, mixer_layer(): jnp.dot(normed, partial_weight, preferred_element_type=jnp.float32)  8.42 us
  transfers between devices with their start and end apart: 4, of which 4 were waited for; matrix products, arithmetic and copies ran while one was open for 4% of the time, Pallas kernels for 0%

commit v1 on v0

v1 whole, which is shorter than its diff:
```python
import functools

import jax
import jax.numpy as jnp
from jax import lax
from jax.experimental import pallas as pl
from jax.experimental.pallas import tpu as pltpu
from jax.sharding import PartitionSpec as P

EPS = 1e-06
MESH = pl.DeviceIdType.MESH
F32 = jnp.float32
BF16 = jnp.bfloat16


def kernel(
    cfg, tok_h, gain, wq_h, wf_h, wv_h, wg_h, floor, hgain, wo_h, st_h,
    mixed_h, new_h,
    cur, w, wo, st, sqs, sqr, part, arecv, psum, brecv, gall, opart, trecv,
    ld_tok, ld_w, ld_wo, ld_st, out_sem, mix_sem,
    sq_s, sq_r, a_s, a_r, b_s, b_r, g_s, g_r, t_s, t_r, u_s, u_r,
):
    layers, n, nt, rows, hd, dk, feat, batch = cfg
    nz = n // 2
    share = batch // nt
    width = hd * dk
    me = lax.axis_index("dp")
    mt = lax.axis_index("tp")
    zme, core = me // 2, lax.rem(me, 2)
    w_h = (wq_h, wf_h, wv_h, wg_h)

    tok_load = pltpu.make_async_copy(tok_h, cur.at[0], ld_tok)
    tok_load.start()
    w_loads = [
        [pltpu.make_async_copy(w_h[p].at[l], w.at[l, p], ld_w.at[l, p]) for p in range(4)]
        for l in range(layers)
    ]
    st_loads = [
        [pltpu.make_async_copy(st_h.at[l, :, h], st.at[l, :, h], ld_st.at[l, h]) for h in range(hd)]
        for l in range(layers)
    ]
    wo_loads = [pltpu.make_async_copy(wo_h.at[l], wo.at[l], ld_wo.at[l]) for l in range(layers)]
    for l in range(layers):
        for p in range(4):
            w_loads[l][p].start()
        for h in range(hd):
            st_loads[l][h].start()
        wo_loads[l].start()

    barrier = pltpu.get_barrier_semaphore()
    for j in range(1, n):
        pl.semaphore_signal(barrier, inc=1, device_id={"dp": lax.rem(me + j, n)}, device_id_type=MESH)
    for j in range(1, nt):
        pl.semaphore_signal(barrier, inc=1, device_id={"tp": lax.rem(mt + j, nt)}, device_id_type=MESH)

    def remote(src, dst, ssem, rsem, dev):
        return pltpu.make_async_remote_copy(
            src_ref=src, dst_ref=dst, send_sem=ssem, recv_sem=rsem, device_id=dev, device_id_type=MESH
        )

    def sq_copy(l, j):
        return remote(sqs.at[l], sqr.at[l, j - 1], sq_s.at[l, j - 1], sq_r.at[l, j - 1],
                      {"dp": lax.rem(me + j, n)})

    def a_copy(l, h):
        return remote(part.at[l, h, :, 1 - core], arecv.at[l, h], a_s.at[l, h], a_r.at[l, h],
                      {"dp": zme * 2 + (1 - core)})

    def b_copy(l, h, j):
        z = lax.rem(zme + j, nz)
        return remote(psum.at[l, h, z], brecv.at[l, h, j - 1], b_s.at[l, h, j - 1], b_r.at[l, h, j - 1],
                      {"dp": z * 2 + core})

    def g_copy(l, j):
        mine = pl.ds(pl.multiple_of(me * rows, rows), rows)
        return remote(gall.at[l, mine], gall.at[l, mine], g_s.at[l, j - 1], g_r.at[l, j - 1],
                      {"dp": lax.rem(me + j, n)})

    def t_copy(l, j):
        t = lax.rem(mt + j, nt)
        return remote(opart.at[l, pl.ds(pl.multiple_of(t * share, share), share)], trecv.at[l, j - 1],
                      t_s.at[l, j - 1], t_r.at[l, j - 1], {"tp": t})

    def u_copy(l, j):
        mine = pl.ds(pl.multiple_of(mt * share, share), share)
        return remote(cur.at[l + 1, mine], cur.at[l + 1, mine], u_s.at[l, j - 1], u_r.at[l, j - 1],
                      {"tp": lax.rem(mt + j, nt)})

    tok_load.wait()
    for l in range(layers):
        tok = cur[l].astype(F32)
        own_sq = jnp.sum(tok * tok, axis=1, keepdims=True)
        eye = lax.broadcasted_iota(jnp.int32, (batch, batch), 0) == lax.broadcasted_iota(
            jnp.int32, (batch, batch), 1)
        sq_row = jnp.sum(jnp.where(eye, own_sq, 0.0), axis=0, keepdims=True)
        sqs[l] = jnp.broadcast_to(sq_row, (8, batch))
        if l == 0:
            pl.semaphore_wait(barrier, n + nt - 2)
        for j in range(1, n):
            sq_copy(l, j).start()
        normed = (tok * gain[l : l + 1, :]).astype(BF16)
        for p in range(4):
            w_loads[l][p].wait()
        for h in range(hd):
            for p in range(4):
                prod = jnp.dot(normed, w[l, p, :, h * dk : (h + 1) * dk], preferred_element_type=F32)
                part[l, h, :, :, :, p * dk : (p + 1) * dk] = prod.astype(BF16).reshape(nz, 2, rows, dk)
            a_copy(l, h).start()

        def pair(h, _, l=l):
            a_copy(l, h).wait_recv()
            total = part[l, h, :, core].astype(F32) + arecv[l, h].astype(F32)
            psum[l, h] = total.astype(BF16)
            for j in range(1, nz):
                b_copy(l, h, j).start()
            return 0

        lax.fori_loop(0, hd, pair, 0)

        sq_all = sqs[l]
        for j in range(1, n):
            sq_copy(l, j).wait_recv()
            sq_all = sq_all + sqr[l, j - 1]
        pick = lax.broadcasted_iota(jnp.int32, (rows, batch), 1) == me * rows + lax.broadcasted_iota(
            jnp.int32, (rows, batch), 0)
        own = jnp.sum(jnp.where(pick, sq_all[0:1, :], 0.0), axis=1, keepdims=True)
        scale = lax.rsqrt(own / (feat * n) + EPS)
        hg = hgain[l : l + 1, :]

        def head(h, _, l=l, scale=scale, hg=hg):
            summed = psum[l, h, zme].astype(F32)
            for j in range(1, nz):
                b_copy(l, h, j).wait_recv()
                summed = summed + brecv[l, h, j - 1].astype(F32)
            stored = (scale * summed).astype(BF16).astype(F32)
            q_pre, f_pre = stored[:, :dk], stored[:, dk : 2 * dk]
            value, g_pre = stored[:, 2 * dk : 3 * dk], stored[:, 3 * dk :]
            query = q_pre * jax.nn.sigmoid(q_pre) * dk ** (-0.5)
            fl = floor[l, pl.ds(h, 1), :]
            forget = fl + (1.0 - fl) * jax.nn.sigmoid(f_pre)
            key_in = (1.0 - fl) * jax.nn.sigmoid(-f_pre)
            stack = [query, forget, key_in]
            pad = -(3 * rows) % 128
            if pad:
                stack.append(jnp.zeros((pad, dk), F32))
            cols = jnp.concatenate(stack, axis=0).T
            pltpu.make_async_copy(st_h.at[l, :, h], st.at[l, :, h], ld_st.at[l, h]).wait()
            reads = []
            for b in range(rows):
                updated = (
                    st[l, b, h] * cols[:, rows + b : rows + b + 1]
                    + cols[:, 2 * rows + b : 2 * rows + b + 1] * value[b : b + 1, :]
                )
                st[l, b, h] = updated
                reads.append(jnp.sum(cols[:, b : b + 1] * updated, axis=0, keepdims=True))
            pltpu.make_async_copy(st.at[l, :, h], new_h.at[l, :, h], out_sem.at[l, h]).start()
            read = jnp.concatenate(reads, axis=0)
            read = read * lax.rsqrt(jnp.mean(read * read, axis=-1, keepdims=True) + EPS) * hg
            gated = (read * (g_pre * jax.nn.sigmoid(g_pre))).astype(BF16)
            gall[l, pl.ds(pl.multiple_of(me * rows, rows), rows),
                 pl.ds(pl.multiple_of(h * dk, dk), dk)] = gated
            return 0

        lax.fori_loop(0, hd, head, 0)

        for j in range(1, n):
            g_copy(l, j).start()
        wo_loads[l].wait()
        for j in range(1, n):
            g_copy(l, j).wait_recv()
        update = jnp.dot(gall[l], wo[l], preferred_element_type=F32)
        opart[l] = update.astype(BF16)
        for j in range(1, nt):
            t_copy(l, j).start()
        mine = pl.ds(pl.multiple_of(mt * share, share), share)
        total = opart[l, mine, :].astype(F32)
        for j in range(1, nt):
            t_copy(l, j).wait_recv()
            total = total + trecv[l, j - 1].astype(F32)
        cur[l + 1, mine, :] = (cur[l, mine, :].astype(F32) + total).astype(BF16)
        for j in range(1, nt):
            u_copy(l, j).start()
        for j in range(1, nt):
            u_copy(l, j).wait_recv()

    mixed = pltpu.make_async_copy(cur.at[layers], mixed_h, mix_sem)
    mixed.start()
    for l in range(layers):
        for j in range(1, n):
            sq_copy(l, j).wait_send()
            g_copy(l, j).wait_send()
        for j in range(1, nt):
            t_copy(l, j).wait_send()
            u_copy(l, j).wait_send()

        def drain(h, _, l=l):
            a_copy(l, h).wait_send()
            for j in range(1, nz):
                b_copy(l, h, j).wait_send()
            pltpu.make_async_copy(st.at[l, :, h], new_h.at[l, :, h], out_sem.at[l, h]).wait()
            return 0

        lax.fori_loop(0, hd, drain, 0)
    mixed.wait()


def per_device(
    n, nt, tokens, norm_gain, w_query, w_forget, w_value, w_gate, floor_rate, head_gain, w_output, state
):
    layers, rows, hd, dk, _ = state.shape
    batch, feat = tokens.shape
    width = hd * dk
    nz = n // 2
    share = batch // nt
    cfg = (layers, n, nt, rows, hd, dk, feat, batch)
    dma = pltpu.SemaphoreType.DMA
    vmem = pl.BlockSpec(memory_space=pltpu.VMEM)
    hbm = pl.BlockSpec(memory_space=pl.ANY)
    mixed, new_state = pl.pallas_call(
        functools.partial(kernel, cfg),
        out_shape=(
            jax.ShapeDtypeStruct(tokens.shape, BF16),
            jax.ShapeDtypeStruct(state.shape, F32),
        ),
        in_specs=[hbm, vmem, hbm, hbm, hbm, hbm, vmem, vmem, hbm, hbm],
        out_specs=(hbm, hbm),
        scratch_shapes=[
            pltpu.VMEM((layers + 1, batch, feat), BF16),
            pltpu.VMEM((layers, 4, feat, width), BF16),
            pltpu.VMEM((layers, width, feat), BF16),
            pltpu.VMEM(state.shape, F32),
            pltpu.VMEM((layers, 8, batch), F32),
            pltpu.VMEM((layers, n - 1, 8, batch), F32),
            pltpu.VMEM((layers, hd, nz, 2, rows, 4 * dk), BF16),
            pltpu.VMEM((layers, hd, nz, rows, 4 * dk), BF16),
            pltpu.VMEM((layers, hd, nz, rows, 4 * dk), BF16),
            pltpu.VMEM((layers, hd, nz - 1, rows, 4 * dk), BF16),
            pltpu.VMEM((layers, batch, width), BF16),
            pltpu.VMEM((layers, batch, feat), BF16),
            pltpu.VMEM((layers, nt - 1, share, feat), BF16),
            dma(()), dma((layers, 4)), dma((layers,)), dma((layers, hd)), dma((layers, hd)), dma(()),
            dma((layers, n - 1)), dma((layers, n - 1)),
            dma((layers, hd)), dma((layers, hd)),
            dma((layers, hd, nz - 1)), dma((layers, hd, nz - 1)),
            dma((layers, n - 1)), dma((layers, n - 1)),
            dma((layers, nt - 1)), dma((layers, nt - 1)),
            dma((layers, nt - 1)), dma((layers, nt - 1)),
        ],
        compiler_params=pltpu.CompilerParams(
            collective_id=0, has_side_effects=True, vmem_limit_bytes=48 * 1024 * 1024
        ),
    )(
        tokens, norm_gain, w_query, w_forget, w_value, w_gate,
        floor_rate.reshape(layers, hd, dk), head_gain, w_output, state,
    )
    return mixed, new_state


def solution(mesh):
    in_specs = (
        P(None, "dp"),
        P(None, "dp"),
        P(None, "dp", "tp"),
        P(None, "dp", "tp"),
        P(None, "dp", "tp"),
        P(None, "dp", "tp"),
        P(None, "tp"),
        P(),
        P(None, "tp", "dp"),
        P(None, "dp", "tp", None, None),
    )
    out_specs = (P(None, "dp"), P(None, "dp", "tp", None, None))
    return jax.shard_map(
        functools.partial(per_device, mesh.shape["dp"], mesh.shape["tp"]),
        mesh=mesh, in_specs=in_specs, out_specs=out_specs, check_vma=False,
    )
```

time: 213 us -> 71.4 us (0.34)
  blocking collectives: 76.9 us -> 0 us
  waiting for transfers between devices: 68.7 us -> 0 us
  Pallas kernels: 0 us -> 52.7 us
  matrix products: 25 us -> 0 us
  other arithmetic: 24.4 us -> 0 us
  local copies, waits for them, and re-layouts: 2.25 us -> 17.6 us
  between operations: 14.8 us -> 0.65 us
    reduce_scatter x4 -> x0, waiting for transfers between devices: 68.6 us -> none  [the longest x2 36.9 us: mixer_layer(): lax.psum_scatter(partial_update.astype(jnp.bfloat16), 'tp', scatter_dimen...]
    pallas_call x0 -> x1, Pallas kernels: none -> 52.7 us  [per_device(): pl.pallas_call(functools.partial(kernel, cfg), out_shape=(jax.ShapeDtypeS...]
    all_gather x4 -> x0, blocking collectives: 44.9 us -> none  [the longest x2 27.9 us: mixer_layer(): lax.all_gather(gated, 'dp', axis=0, tiled=True)]
    unnamed x2 -> x0, blocking collectives: 32 us -> none
    dot_general x12 -> x0, matrix products: 25 us -> none  [the longest x2 13.8 us: mixer_layer(): jnp.einsum('bhk,bhkv->bhv', query, updated, precision=lax.Precision.HIGHEST)]
    unnamed x22 -> x18, local copies, waits for them, and re-layouts: 1.3 us -> 16.9 us
    add x3 -> x0, other arithmetic: 10.4 us -> none  [the longest x1 10.4 us: mixer_layer(): old_state * forget[..., None] + key_in[..., None] * value[:, :, None, :]]
    another operation x1 -> x0, other arithmetic: 7.97 us -> none  [per_device(): return (current, jnp.stack(states, axis=0))]
  transfers between devices with their start and end apart: 4 -> 0, of which waited for: 4 -> 0; matrix products, arithmetic and copies ran while one was open for 4% -> 0% of each run, Pallas kernels for 0% -> 0%
where the time goes in v1:
time: 71.4 us; the launch traced here: 70.9 us
  Pallas kernels  52.7 us (74%)
  local copies, waits for them, and re-layouts  17.6 us (25%)
    pallas_call x1, Pallas kernels, per_device(): pl.pallas_call(functools.partial(kernel, cfg), out_shape=(jax.ShapeDtypeS...  52.7 us
    unnamed x18, local copies, waits for them, and re-layouts  16.9 us

profile of v1, /device:TPU:0, one launch (start us, length us, event | category | flops | bytes accessed | tf_op | source)
XLA Modules:
  0.0 70.9 jit_solution(12813684448088057728)
XLA Ops:
  0.6 0.7 reshape.7.floor
  1.3 0.0 copy-start
  1.3 1.2 %copy-done = bf16[2,512,512]{2,1,0:T(8,128)(2,1)S(1)} copy-done((bf16[2,512,512]{2,1,0:T(8,128)(2,1)S(1)}, bf16[2,512,512]{2,1,0:T(8,128)(2,1)}, u32[]{:S(2)}) %copy-start) | copy-done | bytes 1048600
  2.6 0.0 copy-start.1
  2.6 1.2 %copy-done.1 = bf16[2,512,512]{2,1,0:T(8,128)(2,1)S(1)} copy-done((bf16[2,512,512]{2,1,0:T(8,128)(2,1)S(1)}, bf16[2,512,512]{2,1,0:T(8,128)(2,1)}, u32[]{:S(2)}) %copy-start.1) | copy-done | bytes 1048600
  3.8 0.0 copy-start.2
  3.8 1.2 %copy-done.2 = bf16[2,512,512]{2,1,0:T(8,128)(2,1)S(1)} copy-done((bf16[2,512,512]{2,1,0:T(8,128)(2,1)S(1)}, bf16[2,512,512]{2,1,0:T(8,128)(2,1)}, u32[]{:S(2)}) %copy-start.2) | copy-done | bytes 1048600
  5.0 0.0 copy-start.3
  5.0 1.2 %copy-done.3 = bf16[2,512,512]{2,1,0:T(8,128)(2,1)S(1)} copy-done((bf16[2,512,512]{2,1,0:T(8,128)(2,1)S(1)}, bf16[2,512,512]{2,1,0:T(8,128)(2,1)}, u32[]{:S(2)}) %copy-start.3) | copy-done | bytes 1048600
  6.2 0.0 copy-start.4
  6.2 1.2 %copy-done.4 = bf16[2,512,512]{2,1,0:T(8,128)(2,1)S(1)} copy-done((bf16[2,512,512]{2,1,0:T(8,128)(2,1)S(1)}, bf16[2,512,512]{2,1,0:T(8,128)(2,1)}, u32[]{:S(2)}) %copy-start.4) | copy-done | bytes 1048600
  7.5 0.0 copy-start.5
  7.5 0.9 %copy-done.5 = bf16[128,512]{1,0:T(8,128)(2,1)S(1)} copy-done((bf16[128,512]{1,0:T(8,128)(2,1)S(1)}, bf16[128,512]{1,0:T(8,128)(2,1)}, u32[]{:S(2)}) %copy-start.5) | copy-done | bytes 131096
  8.4 0.0 copy-start.6
  8.4 0.7 copy-done.6
  9.0 0.0 copy-start.7
  9.1 0.7 copy-done.7
  9.7 52.7 %shard_map.113 = (bf16[128,512]{1,0:T(8,128)(2,1)S(1)}, f32[2,16,4,128,128]{4,3,2,1,0:T(8,128)}) custom-call(bf16[128,512]{1,0:T(8,128)(2,1)S(1)} %copy-done.5, f32[2,512]{1,0:T(2,128)S(1)} %copy-done.6, bf16[2,512,512]{2,1,0:T(8,128)(2,1)S(1)} %copy-done, bf16[2,512,512]{2,1,0:T(8,128)(2,1)S(1)} %copy-done.1, bf16[2,512,512]{2,1,0:T(8,128)(2,1)S(1)} %copy-done.2, ...), custom_call_target="tpu_custom_call" | custom-call | tf_op jit(solution)/shard_map/pallas_call | solution.py:219
  62.4 0.7 copy.14
  63.0 7.9 %copy.15 = f32[2,16,4,128,128]{4,3,2,1,0:T(8,128)} copy(f32[2,16,4,128,128]{4,3,2,1,0:T(8,128)} %get-tuple-element.5) | data formatting | bytes 16777216
Async XLA Ops:
  1.3 1.2 %copy-start = (bf16[2,512,512]{2,1,0:T(8,128)(2,1)S(1)}, bf16[2,512,512]{2,1,0:T(8,128)(2,1)}, u32[]{:S(2)}) copy-start(bf16[2,512,512]{2,1,0:T(8,128)(2,1)} %wq_h.1) | copy-start | bytes 3145732
  2.6 1.2 %copy-start.1 = (bf16[2,512,512]{2,1,0:T(8,128)(2,1)S(1)}, bf16[2,512,512]{2,1,0:T(8,128)(2,1)}, u32[]{:S(2)}) copy-start(bf16[2,512,512]{2,1,0:T(8,128)(2,1)} %wf_h.1) | copy-start | bytes 3145732
  3.8 1.2 %copy-start.2 = (bf16[2,512,512]{2,1,0:T(8,128)(2,1)S(1)}, bf16[2,512,512]{2,1,0:T(8,128)(2,1)}, u32[]{:S(2)}) copy-start(bf16[2,512,512]{2,1,0:T(8,128)(2,1)} %wv_h.1) | copy-start | bytes 3145732
  5.0 1.2 %copy-start.3 = (bf16[2,512,512]{2,1,0:T(8,128)(2,1)S(1)}, bf16[2,512,512]{2,1,0:T(8,128)(2,1)}, u32[]{:S(2)}) copy-start(bf16[2,512,512]{2,1,0:T(8,128)(2,1)} %wg_h.1) | copy-start | bytes 3145732
  6.2 1.2 %copy-start.4 = (bf16[2,512,512]{2,1,0:T(8,128)(2,1)S(1)}, bf16[2,512,512]{2,1,0:T(8,128)(2,1)}, u32[]{:S(2)}) copy-start(bf16[2,512,512]{2,1,0:T(8,128)(2,1)} %wo_h.1) | copy-start | bytes 3145732
  7.5 0.9 %copy-start.5 = (bf16[128,512]{1,0:T(8,128)(2,1)S(1)}, bf16[128,512]{1,0:T(8,128)(2,1)}, u32[]{:S(2)}) copy-start(bf16[128,512]{1,0:T(8,128)(2,1)} %tok_h.1) | copy-start | bytes 393220
  8.4 0.7 copy-start.6
  9.0 0.7 copy-start.7

commit v2 on v1

v2 whole, which is shorter than its diff:
```python
import functools

import jax
import jax.numpy as jnp
from jax import lax
from jax.experimental import pallas as pl
from jax.experimental.pallas import tpu as pltpu
from jax.sharding import PartitionSpec as P

EPS = 1e-06
MESH = pl.DeviceIdType.MESH
F32 = jnp.float32
BF16 = jnp.bfloat16


def kernel(
    cfg, tok_h, gain_h, wq_h, wf_h, wv_h, wg_h, floor_h, hgain_h, wo_h, st_h,
    mixed, st,
    cur, gain, floor, hgain, w, wo, colbuf, valbuf, sqs, sqr, part, arecv, psum, brecv, gall, opart, trecv,
    ld_tok, ld_w, ld_wo, ld_st, ld_small,
    sq_s, sq_r, a_s, a_r, b_s, b_r, g_s, g_r, t_s, t_r, u_s, u_r,
):
    layers, n, nt, rows, hd, dk, feat, batch, nc = cfg
    part_feat = feat // nc
    nz = n // 2
    share = batch // nt
    width = hd * dk
    me = lax.axis_index("dp")
    mt = lax.axis_index("tp")
    zme, core = me // 2, lax.rem(me, 2)
    w_h = (wq_h, wf_h, wv_h, wg_h)

    tok_loads = [
        pltpu.make_async_copy(tok_h.at[:, pl.ds(c * part_feat, part_feat)], cur.at[0, c], ld_tok.at[c])
        for c in range(nc)
    ]
    small = [
        pltpu.make_async_copy(src, dst, ld_small.at[i])
        for i, (src, dst) in enumerate(((gain_h, gain), (floor_h, floor), (hgain_h, hgain)))
    ]
    for load in tok_loads + small:
        load.start()
    w_loads = [
        [pltpu.make_async_copy(w_h[p].at[l], w.at[l, p], ld_w.at[l, p]) for p in range(4)]
        for l in range(layers)
    ]
    st_loads = [
        [pltpu.make_async_copy(st_h.at[l, :, h], st.at[l, :, h], ld_st.at[l, h]) for h in range(hd)]
        for l in range(layers)
    ]
    wo_loads = [pltpu.make_async_copy(wo_h.at[l], wo.at[l], ld_wo.at[l]) for l in range(layers)]
    for load in w_loads[0]:
        load.start()

    barrier = pltpu.get_barrier_semaphore()
    for j in range(1, n):
        pl.semaphore_signal(barrier, inc=1, device_id={"dp": lax.rem(me + j, n)}, device_id_type=MESH)
    for j in range(1, nt):
        pl.semaphore_signal(barrier, inc=1, device_id={"tp": lax.rem(mt + j, nt)}, device_id_type=MESH)

    def remote(src, dst, ssem, rsem, dev):
        return pltpu.make_async_remote_copy(
            src_ref=src, dst_ref=dst, send_sem=ssem, recv_sem=rsem, device_id=dev, device_id_type=MESH
        )

    def whole(l):
        return jnp.concatenate([cur[l, c] for c in range(nc)], axis=1)

    def sq_copy(l, j):
        return remote(sqs.at[l], sqr.at[l, j - 1], sq_s.at[l, j - 1], sq_r.at[l, j - 1],
                      {"dp": lax.rem(me + j, n)})

    def a_copy(l, h):
        return remote(part.at[l, h, :, 1 - core], arecv.at[l, h], a_s.at[l, h], a_r.at[l, h],
                      {"dp": zme * 2 + (1 - core)})

    def b_copy(l, h, j):
        z = lax.rem(zme + j, nz)
        return remote(psum.at[l, h, z], brecv.at[l, h, j - 1], b_s.at[l, h, j - 1], b_r.at[l, h, j - 1],
                      {"dp": z * 2 + core})

    def g_copy(l, h, j):
        mine = pl.ds(pl.multiple_of(me * rows, rows), rows)
        return remote(gall.at[l, h, mine], gall.at[l, h, mine], g_s.at[l, h, j - 1], g_r.at[l, h, j - 1],
                      {"dp": lax.rem(me + j, n)})

    def t_copy(l, c, j):
        t = lax.rem(mt + j, nt)
        return remote(opart.at[l, c, pl.ds(pl.multiple_of(t * share, share), share)], trecv.at[l, c, j - 1],
                      t_s.at[l, c, j - 1], t_r.at[l, c, j - 1], {"tp": t})

    def u_copy(l, c, j):
        mine = pl.ds(pl.multiple_of(mt * share, share), share)
        return remote(cur.at[l + 1, c, mine], cur.at[l + 1, c, mine], u_s.at[l, c, j - 1], u_r.at[l, c, j - 1],
                      {"tp": lax.rem(mt + j, nt)})

    for load in tok_loads + small:
        load.wait()
    for l in range(layers):
        tok = whole(l).astype(F32)
        own_sq = jnp.sum(tok * tok, axis=1, keepdims=True)
        eye = lax.broadcasted_iota(jnp.int32, (batch, batch), 0) == lax.broadcasted_iota(
            jnp.int32, (batch, batch), 1)
        sq_row = jnp.sum(jnp.where(eye, own_sq, 0.0), axis=0, keepdims=True)
        sqs[l] = jnp.broadcast_to(sq_row, (8, batch))
        if l == 0:
            pl.semaphore_wait(barrier, n + nt - 2)
        for j in range(1, n):
            sq_copy(l, j).start()
        normed = (tok * gain[l : l + 1, :]).astype(BF16)
        for p in range(4):
            w_loads[l][p].wait()
        if l == 0:
            for load in st_loads[0] + [wo_loads[0]]:
                load.start()
        for h in range(hd):
            for p in range(4):
                prod = jnp.dot(normed, w[l, p, :, h * dk : (h + 1) * dk], preferred_element_type=F32)
                part[l, h, :, :, :, p * dk : (p + 1) * dk] = prod.astype(BF16).reshape(nz, 2, rows, dk)
            a_copy(l, h).start()

        def pair(h, _, l=l):
            a_copy(l, h).wait_recv()
            total = part[l, h, :, core].astype(F32) + arecv[l, h].astype(F32)
            psum[l, h] = total.astype(BF16)
            for j in range(1, nz):
                b_copy(l, h, j).start()
            return 0

        lax.fori_loop(0, hd, pair, 0)

        sq_all = sqs[l]
        for j in range(1, n):
            sq_copy(l, j).wait_recv()
            sq_all = sq_all + sqr[l, j - 1]
        pick = lax.broadcasted_iota(jnp.int32, (rows, batch), 1) == me * rows + lax.broadcasted_iota(
            jnp.int32, (rows, batch), 0)
        own = jnp.sum(jnp.where(pick, sq_all[0:1, :], 0.0), axis=1, keepdims=True)
        scale = lax.rsqrt(own / (feat * n) + EPS)
        hg = hgain[l : l + 1, :]

        def head(h, _, l=l, scale=scale, hg=hg):
            summed = psum[l, h, zme].astype(F32)
            for j in range(1, nz):
                b_copy(l, h, j).wait_recv()
                summed = summed + brecv[l, h, j - 1].astype(F32)
            stored = (scale * summed).astype(BF16).astype(F32)
            q_pre, f_pre = stored[:, :dk], stored[:, dk : 2 * dk]
            value, g_pre = stored[:, 2 * dk : 3 * dk], stored[:, 3 * dk :]
            query = q_pre * jax.nn.sigmoid(q_pre) * dk ** (-0.5)
            fl = floor[l : l + 1, pl.ds(pl.multiple_of(h * dk, dk), dk)]
            forget = fl + (1.0 - fl) * jax.nn.sigmoid(f_pre)
            key_in = (1.0 - fl) * jax.nn.sigmoid(-f_pre)
            stack = [query * forget, forget, key_in]
            pad = -(3 * rows) % 128
            if pad:
                stack.append(jnp.zeros((pad, dk), F32))
            cols = jnp.concatenate(stack, axis=0).T
            pltpu.make_async_copy(st_h.at[l, :, h], st.at[l, :, h], ld_st.at[l, h]).wait()
            colbuf[h] = cols
            valbuf[h] = value
            reads = [
                jnp.sum(cols[:, b : b + 1] * st[l, b, h], axis=0, keepdims=True) for b in range(rows)
            ]
            along = jnp.sum(query * key_in, axis=-1, keepdims=True)
            read = jnp.concatenate(reads, axis=0) + along * value
            read = read * lax.rsqrt(jnp.mean(read * read, axis=-1, keepdims=True) + EPS) * hg
            gated = (read * (g_pre * jax.nn.sigmoid(g_pre))).astype(BF16)
            gall[l, h, pl.ds(pl.multiple_of(me * rows, rows), rows), :] = gated
            for j in range(1, n):
                g_copy(l, h, j).start()
            return 0

        lax.fori_loop(0, hd, head, 0)

        if l + 1 < layers:
            for load in w_loads[l + 1] + st_loads[l + 1] + [wo_loads[l + 1]]:
                load.start()

        def renew(h, _, l=l):
            cols, value = colbuf[h], valbuf[h]
            for b in range(rows):
                st[l, b, h] = (
                    st[l, b, h] * cols[:, rows + b : rows + b + 1]
                    + cols[:, 2 * rows + b : 2 * rows + b + 1] * value[b : b + 1, :]
                )
            return 0

        lax.fori_loop(0, hd, renew, 0)

        wo_loads[l].wait()
        for h in range(hd):
            for j in range(1, n):
                g_copy(l, h, j).wait_recv()
        gathered = jnp.concatenate([gall[l, h] for h in range(hd)], axis=1)
        for c in range(nc):
            cols = slice(c * part_feat, (c + 1) * part_feat)
            update = jnp.dot(gathered, wo[l, :, cols], preferred_element_type=F32)
            opart[l, c] = update.astype(BF16)
            for j in range(1, nt):
                t_copy(l, c, j).start()
        mine = pl.ds(pl.multiple_of(mt * share, share), share)
        for c in range(nc):
            cols = slice(c * part_feat, (c + 1) * part_feat)
            total = opart[l, c, mine, :].astype(F32)
            for j in range(1, nt):
                t_copy(l, c, j).wait_recv()
                total = total + trecv[l, c, j - 1].astype(F32)
            cur[l + 1, c, mine, :] = (cur[l, c, mine, :].astype(F32) + total).astype(BF16)
            for j in range(1, nt):
                u_copy(l, c, j).start()
        for c in range(nc):
            for j in range(1, nt):
                u_copy(l, c, j).wait_recv()

    mixed[...] = whole(layers)
    for l in range(layers):
        for j in range(1, n):
            sq_copy(l, j).wait_send()
        for c in range(nc):
            for j in range(1, nt):
                t_copy(l, c, j).wait_send()
                u_copy(l, c, j).wait_send()

        def drain(h, _, l=l):
            a_copy(l, h).wait_send()
            for j in range(1, nz):
                b_copy(l, h, j).wait_send()
            for j in range(1, n):
                g_copy(l, h, j).wait_send()
            return 0

        lax.fori_loop(0, hd, drain, 0)


def flush(mixed, st, mixed_h, new_h, st_sem, mix_sem):
    copies = [
        pltpu.make_async_copy(st.at[l, :, h], new_h.at[l, :, h], st_sem.at[l, h])
        for l in range(st.shape[0])
        for h in range(st.shape[2])
    ]
    copies.append(pltpu.make_async_copy(mixed, mixed_h, mix_sem))
    for copy in copies:
        copy.start()
    for copy in copies:
        copy.wait()


def per_device(
    n, nt, tokens, norm_gain, w_query, w_forget, w_value, w_gate, floor_rate, head_gain, w_output, state
):
    layers, rows, hd, dk, _ = state.shape
    batch, feat = tokens.shape
    width = hd * dk
    nz = n // 2
    share = batch // nt
    nc = 2
    cfg = (layers, n, nt, rows, hd, dk, feat, batch, nc)
    dma = pltpu.SemaphoreType.DMA
    vmem = pl.BlockSpec(memory_space=pltpu.VMEM)
    hbm_or_vmem = pl.BlockSpec(memory_space=pl.ANY)
    hbm = pl.BlockSpec(memory_space=pltpu.HBM)
    mixed, new_state = pl.pallas_call(
        functools.partial(kernel, cfg),
        out_shape=(
            jax.ShapeDtypeStruct(tokens.shape, BF16),
            jax.ShapeDtypeStruct(state.shape, F32),
        ),
        in_specs=[hbm] * 10,
        out_specs=(vmem, vmem),
        scratch_shapes=[
            pltpu.VMEM((layers + 1, nc, batch, feat // nc), BF16),
            pltpu.VMEM(norm_gain.shape, F32),
            pltpu.VMEM(floor_rate.shape, F32),
            pltpu.VMEM(head_gain.shape, F32),
            pltpu.VMEM((layers, 4, feat, width), BF16),
            pltpu.VMEM((layers, width, feat), BF16),
            pltpu.VMEM((hd, dk, -(-3 * rows // 128) * 128), F32),
            pltpu.VMEM((hd, rows, dk), F32),
            pltpu.VMEM((layers, 8, batch), F32),
            pltpu.VMEM((layers, n - 1, 8, batch), F32),
            pltpu.VMEM((layers, hd, nz, 2, rows, 4 * dk), BF16),
            pltpu.VMEM((layers, hd, nz, rows, 4 * dk), BF16),
            pltpu.VMEM((layers, hd, nz, rows, 4 * dk), BF16),
            pltpu.VMEM((layers, hd, nz - 1, rows, 4 * dk), BF16),
            pltpu.VMEM((layers, hd, batch, dk), BF16),
            pltpu.VMEM((layers, nc, batch, feat // nc), BF16),
            pltpu.VMEM((layers, nc, nt - 1, share, feat // nc), BF16),
            dma((nc,)), dma((layers, 4)), dma((layers,)), dma((layers, hd)), dma((3,)),
            dma((layers, n - 1)), dma((layers, n - 1)),
            dma((layers, hd)), dma((layers, hd)),
            dma((layers, hd, nz - 1)), dma((layers, hd, nz - 1)),
            dma((layers, hd, n - 1)), dma((layers, hd, n - 1)),
            dma((layers, nc, nt - 1)), dma((layers, nc, nt - 1)),
            dma((layers, nc, nt - 1)), dma((layers, nc, nt - 1)),
        ],
        compiler_params=pltpu.CompilerParams(
            collective_id=0, has_side_effects=True, vmem_limit_bytes=36 * 1024 * 1024
        ),
    )(
        *(
            pltpu.with_memory_space_constraint(array, pltpu.HBM)
            for array in (
                tokens, norm_gain, w_query, w_forget, w_value, w_gate,
                floor_rate, head_gain, w_output, state,
            )
        )
    )
    return pl.pallas_call(
        flush,
        out_shape=(
            jax.ShapeDtypeStruct(tokens.shape, BF16),
            jax.ShapeDtypeStruct(state.shape, F32),
        ),
        in_specs=[hbm_or_vmem, hbm_or_vmem],
        out_specs=(hbm, hbm),
        scratch_shapes=[dma((layers, hd)), dma(())],
        compiler_params=pltpu.CompilerParams(vmem_limit_bytes=1024 * 1024),
    )(mixed, new_state)


def solution(mesh):
    in_specs = (
        P(None, "dp"),
        P(None, "dp"),
        P(None, "dp", "tp"),
        P(None, "dp", "tp"),
        P(None, "dp", "tp"),
        P(None, "dp", "tp"),
        P(None, "tp"),
        P(),
        P(None, "tp", "dp"),
        P(None, "dp", "tp", None, None),
    )
    out_specs = (P(None, "dp"), P(None, "dp", "tp", None, None))
    return jax.shard_map(
        functools.partial(per_device, mesh.shape["dp"], mesh.shape["tp"]),
        mesh=mesh, in_specs=in_specs, out_specs=out_specs, check_vma=False,
    )
```

time: 71.4 us -> 55.1 us (0.77)
  local copies, waits for them, and re-layouts: 17.6 us -> 0 us
  Pallas kernels: 52.7 us -> 54.3 us
    unnamed x18 -> x0, local copies, waits for them, and re-layouts: 16.9 us -> none
    pallas_call x0 -> x1, Pallas kernels: none -> 3.38 us  [per_device(): pl.pallas_call(flush, out_shape=(jax.ShapeDtypeStruct(tokens.shape, BF16)...]
    pallas_call x1, Pallas kernels: 52.7 us -> 50.9 us  [per_device(): pl.pallas_call(functools.partial(kernel, cfg), out_shape=(jax.ShapeDtypeS...]
where the time goes in v2:
time: 55.1 us; the launch traced here: 54.9 us
  Pallas kernels  54.3 us (99%)
  between operations  0.64 us (1%)
    pallas_call x1, Pallas kernels, per_device(): pl.pallas_call(functools.partial(kernel, cfg), out_shape=(jax.ShapeDtypeS...  50.9 us
    pallas_call x1, Pallas kernels, per_device(): pl.pallas_call(flush, out_shape=(jax.ShapeDtypeStruct(tokens.shape, BF16)...  3.38 us

profile of v2, /device:TPU:0, one launch (start us, length us, event | category | flops | bytes accessed | tf_op | source)
XLA Modules:
  0.0 54.9 jit_solution(2605703505158217223)
XLA Ops:
  0.6 50.9 %shard_map.113 = (bf16[128,512]{1,0:T(8,128)(2,1)S(1)}, f32[2,16,4,128,128]{4,3,2,1,0:T(8,128)S(1)}) custom-call(bf16[128,512]{1,0:T(8,128)(2,1)} %tok_h.1, f32[2,512]{1,0:T(2,128)} %gain_h.1, bf16[2,512,512]{2,1,0:T(8,128)(2,1)} %wq_h.1, bf16[2,512,512]{2,1,0:T(8,128)(2,1)} %wf_h.1, bf16[2,512,512]{2,1,0:T(8,128)(2,1)} %wv_h.1, bf16[2,512,512]{2,1,0:T(8,128)(2,1)} %wg_h.1, ...), custom_call_target="tpu_custom_call" | custom-call | tf_op jit(solution)/shard_map/pallas_call | solution.py:263
  51.5 3.4 %shard_map.114 = (bf16[128,512]{1,0:T(8,128)(2,1)}, f32[2,16,4,128,128]{4,3,2,1,0:T(8,128)}) custom-call(bf16[128,512]{1,0:T(8,128)(2,1)S(1)} %get-tuple-element.4.mixed, f32[2,16,4,128,128]{4,3,2,1,0:T(8,128)S(1)} %get-tuple-element.5.st), custom_call_target="tpu_custom_call" | custom-call | tf_op jit(solution)/shard_map/pallas_call | solution.py:309
